TPU v7x, 32 devices: a whole 2x2x4 slice. The times are simulated.
32 devices in a mesh: grp: 2 (over y), fs: 4 (over z), tp: 4 (over x, core).
Axes of the slice: x: 2, y: 2, z: 4, core: 2. Of those that a mesh axis runs over, the one named last changes fastest.
Arguments:
- stream: bfloat16 [2048, 3072], P('tp', ('grp', 'fs')), parts along dimension 1, may hold values from -6 to 6
- mixer_gain: float32 [2048], replicated, may hold values from 0.1 to 1.9
- glu_value: bfloat16 [2048, 1024], P('fs', 'tp'), may hold values from -0.125 to 0.125
- glu_gate: bfloat16 [2048, 1024], P('fs', 'tp'), may hold values from -0.125 to 0.125
- conv_kernel: bfloat16 [31, 1024], replicated, may hold values from -1 to 1
- channel_gain: float32 [1024], replicated, may hold values from 0.1 to 1.9
- conv_out: bfloat16 [2048, 1024], P('fs', 'tp'), may hold values from -0.1875 to 0.1875
- ffn_gain: float32 [2048], replicated, may hold values from 0.1 to 1.9
- ffn_gate: bfloat16 [2048, 5632], P('fs', 'tp'), may hold values from -0.125 to 0.125
- ffn_up: bfloat16 [2048, 5632], P('fs', 'tp'), may hold values from -0.125 to 0.125
- ffn_down: bfloat16 [2048, 5632], P('fs', 'tp'), may hold values from -0.078125 to 0.078125
Outputs:
- result: bfloat16 [2048, 3072], P('tp', ('grp', 'fs')), parts along dimension 1
There are 2 independent parts, one for each index of `grp`. A program takes and returns all parts, laid end to end along the dimension named above; an argument that names none is the same for every part. Nothing has to cross between parts.
All inputs are finite; a program needn't handle non-finite values.
Results may differ from a plain program's by a relative error of at most 0.018.
Values may be sent and summed in bfloat16 or wider, within the bound.
A program may use at most 64 MiB of HBM per device.

v0:
```python
import jax
import jax.numpy as jnp
from jax import lax
from jax.sharding import PartitionSpec as P


def rms_normalize(wide, gain):
    inverse = lax.rsqrt(jnp.mean(wide * wide, axis=0, keepdims=True) + 1e-06)
    return (wide * inverse * gain[:, None]).astype(jnp.bfloat16)


def contract(weight, acts):
    return lax.dot_general(
        weight, acts, (((0,), (0,)), ((), ())), preferred_element_type=jnp.float32
    )


def on_device(
    stream,
    mixer_gain,
    glu_value,
    glu_gate,
    conv_kernel,
    channel_gain,
    conv_out,
    ffn_gain,
    ffn_gate,
    ffn_up,
    ffn_down,
):
    length = stream.shape[1]
    channels = glu_value.shape[1]
    position = lax.axis_index("tp")
    total_channels = channels * lax.axis_size("tp")
    taps = lax.dynamic_slice_in_dim(conv_kernel, position * channels, channels, 1).astype(
        jnp.float32
    )
    gain_local = lax.dynamic_slice_in_dim(channel_gain, position * channels, channels, 0)
    gathered = lax.all_gather(stream, "tp", axis=0, tiled=True)
    normed = rms_normalize(gathered.astype(jnp.float32), mixer_gain)
    value_w, gate_w, out_w = (
        lax.all_gather(glu_value, "fs", axis=0, tiled=True),
        lax.all_gather(glu_gate, "fs", axis=0, tiled=True),
        lax.all_gather(conv_out, "fs", axis=0, tiled=True),
    )
    value_part = contract(value_w, normed)
    gate_part = contract(gate_w, normed)
    gated = (value_part * jax.nn.sigmoid(gate_part)).astype(jnp.bfloat16).astype(jnp.float32)
    padded = jnp.pad(gated, ((0, 0), (taps.shape[0] - 1, 0)))
    conv_sum = jnp.zeros_like(gated)
    for step in range(taps.shape[0]):
        conv_sum = conv_sum + taps[step][:, None] * padded[:, step : step + length]
    sums, squares = lax.psum(
        (jnp.sum(conv_sum, axis=0), jnp.sum(conv_sum * conv_sum, axis=0)), "tp"
    )
    mean_val = sums / total_channels
    mean_sq = squares / total_channels
    scaled = (
        (conv_sum - mean_val[None, :])
        * lax.rsqrt(mean_sq - mean_val * mean_val + 1e-05)[None, :]
        * gain_local[:, None]
    )
    activated = jax.nn.silu(scaled).astype(jnp.bfloat16)
    mixed_sum = lax.psum_scatter(
        jnp.dot(out_w, activated, preferred_element_type=jnp.float32).astype(jnp.bfloat16),
        "tp",
        scatter_dimension=0,
        tiled=True,
    ).astype(jnp.float32)
    middle_wide = stream.astype(jnp.float32) + mixed_sum
    middle = middle_wide.astype(jnp.bfloat16)
    gathered_two = lax.all_gather(middle, "tp", axis=0, tiled=True)
    normed_two = rms_normalize(gathered_two.astype(jnp.float32), ffn_gain)
    gate_whole, up_whole = (
        lax.all_gather(ffn_gate, "fs", axis=0, tiled=True),
        lax.all_gather(ffn_up, "fs", axis=0, tiled=True),
    )
    gate_val = contract(gate_whole, normed_two)
    up_val = contract(up_whole, normed_two)
    hidden = (jax.nn.silu(gate_val) * up_val).astype(jnp.bfloat16)
    down_whole = lax.all_gather(ffn_down, "fs", axis=0, tiled=True)
    ffn_sum = lax.psum_scatter(
        jnp.dot(down_whole, hidden, preferred_element_type=jnp.float32).astype(jnp.bfloat16),
        "tp",
        scatter_dimension=0,
        tiled=True,
    ).astype(jnp.float32)
    return (middle.astype(jnp.float32) + ffn_sum).astype(jnp.bfloat16)


def solution(mesh):
    in_specs = (
        P("tp", ("grp", "fs")),
        P(),
        P("fs", "tp"),
        P("fs", "tp"),
        P(),
        P(),
        P("fs", "tp"),
        P(),
        P("fs", "tp"),
        P("fs", "tp"),
        P("fs", "tp"),
    )
    out_specs = P("tp", ("grp", "fs"))
    return jax.shard_map(
        on_device, mesh=mesh, in_specs=in_specs, out_specs=out_specs, check_vma=False
    )
```

profile of v0, /device:TPU:0, one launch (start us, length us, event | category | flops | bytes accessed | tf_op | source)
XLA Modules:
  0.0 538.9 jit_solution(6192163965069522078)
XLA Ops:
  6.5 0.7 all-gather.9.cloned.1.call-update
  7.3 0.7 all-gather.13.cloned.1.call-update
  8.1 0.7 all-gather.11.cloned.1.call-update
  8.8 0.5 all-gather.15.cloned.1.call-update
  9.4 0.7 dynamic-slice_convert_fusion
  10.1 0.8 dynamic_slice.7
  10.9 20.4 %all-gather.9.cloned.1.call-done = bf16[2048,384]{1,0:T(8,128)(2,1)} async-done(((bf16[512,384]{1,0:T(8,128)(2,1)}), bf16[2048,384]{1,0:T(8,128)(2,1)}) %all-gather.9.cloned.1.call-update) | async-done | bytes 1572880 | tf_op jit(solution)/shard_map/all_gather | solution.py:39
  31.3 1.8 fusion
  33.1 27.8 %all-gather.13.cloned.1.call-done = bf16[2048,256]{1,0:T(8,128)(2,1)} async-done(((bf16[512,256]{1,0:T(8,128)(2,1)}), bf16[2048,256]{1,0:T(8,128)(2,1)}) %all-gather.13.cloned.1.call-update) | async-done | bytes 1048592 | tf_op jit(solution)/shard_map/all_gather | solution.py:43
  60.9 2.7 fusion.12
  63.6 26.2 %all-gather.11.cloned.1.call-done = bf16[2048,256]{1,0:T(8,128)(2,1)} async-done(((bf16[512,256]{1,0:T(8,128)(2,1)}), bf16[2048,256]{1,0:T(8,128)(2,1)}) %all-gather.11.cloned.1.call-update) | async-done | bytes 1048592 | tf_op jit(solution)/shard_map/all_gather | solution.py:42
  89.8 2.2 fusion.15
  92.1 1.6 fusion.76
  93.7 6.1 %all-reduce.1 = (f32[384]{0:T(512)S(1)}, f32[384]{0:T(512)S(1)}) all-reduce(f32[384]{0:T(512)S(1)} %get-tuple-element.6, f32[384]{0:T(512)S(1)} %get-tuple-element.5), channel_id=1, replica_groups=mesh['grp'=2,'fs'=4,'tp'=4] {'tp'}, use_global_device_ids=true, to_apply=%region_4.5 | all-reduce | flops 768 | bytes 6144 | tf_op jit(solution)/shard_map/psum | solution.py:53
  99.8 18.9 %all-gather.15.cloned.1.call-done = bf16[2048,256]{1,0:T(8,128)(2,1)} async-done(((bf16[512,256]{1,0:T(8,128)(2,1)}), bf16[2048,256]{1,0:T(8,128)(2,1)}) %all-gather.15.cloned.1.call-update) | async-done | bytes 1048592 | tf_op jit(solution)/shard_map/all_gather | solution.py:44
  118.7 3.1 fusion.8
  121.8 0.2 copy.12
  122.0 27.2 %reduce-scatter.3.cloned.1.call-done = bf16[512,384]{0,1:T(8,128)(2,1)} async-done(((bf16[2048,384]{0,1:T(8,128)(2,1)}), bf16[512,384]{0,1:T(8,128)(2,1)}) %reduce-scatter.3.cloned.1.call-update) | async-done | bytes 393232 | tf_op jit(solution)/shard_map/reduce_scatter | solution.py:64
  149.3 1.8 add_convert_fusion.1
  151.2 0.7 all-gather.19.cloned.1.call-update
  151.9 0.7 all-gather.21.cloned.1.call-update
  152.7 0.7 all-gather.23.cloned.1.call-update
  153.4 17.5 %all-gather.17.cloned.1.call-done = bf16[2048,384]{0,1:T(8,128)(2,1)} async-done(((bf16[512,384]{0,1:T(8,128)(2,1)}), bf16[2048,384]{0,1:T(8,128)(2,1)}) %all-gather.17.cloned.1.call-update) | async-done | bytes 1572880 | tf_op jit(solution)/shard_map/all_gather | solution.py:72
  170.9 1.8 fusion.3
  172.7 106.5 %all-gather.19.cloned.1.call-done = bf16[2048,1408]{1,0:T(8,128)(2,1)} async-done(((bf16[512,1408]{1,0:T(8,128)(2,1)}), bf16[2048,1408]{1,0:T(8,128)(2,1)}) %all-gather.19.cloned.1.call-update) | async-done | bytes 5767184 | tf_op jit(solution)/shard_map/all_gather | solution.py:75
  279.2 7.1 %convolution_bitcast_fusion.1 = f32[1408,384]{0,1:T(8,128)} fusion(bf16[2048,1408]{1,0:T(8,128)(2,1)} %all-gather.19.cloned.1.call-done, bf16[2048,384]{0,1:T(8,128)(2,1)} %all-gather.17.cloned.1.call-done, f32[2048]{0:T(1024)S(1)} %copy-done.5, f32[384]{0:T(512)S(1)} %add_rsqrt_fusion), kind=kOutput, calls=%fused_computation.12 | convolution fusion | flops 2217738240 | bytes 9512448 | tf_op jit(solution)/shard_map/dot_general | solution.py:13
  286.4 99.4 %all-gather.21.cloned.1.call-done = bf16[2048,1408]{1,0:T(8,128)(2,1)} async-done(((bf16[512,1408]{1,0:T(8,128)(2,1)}), bf16[2048,1408]{1,0:T(8,128)(2,1)}) %all-gather.21.cloned.1.call-update) | async-done | bytes 5767184 | tf_op jit(solution)/shard_map/all_gather | solution.py:76
  385.8 106.6 %all-gather.23.cloned.1.call-done = bf16[2048,1408]{1,0:T(8,128)(2,1)} async-done(((bf16[512,1408]{1,0:T(8,128)(2,1)}), bf16[2048,1408]{1,0:T(8,128)(2,1)}) %all-gather.23.cloned.1.call-update) | async-done | bytes 5767184 | tf_op jit(solution)/shard_map/all_gather | solution.py:81
  492.3 11.3 %fusion.9 = bf16[2048,384]{0,1:T(8,128)(2,1)} fusion(bf16[2048,1408]{1,0:T(8,128)(2,1)} %all-gather.23.cloned.1.call-done, bf16[2048,1408]{1,0:T(8,128)(2,1)} %all-gather.21.cloned.1.call-done, f32[1408,384]{0,1:T(8,128)} %convolution_bitcast_fusion.1, bf16[2048,384]{0,1:T(8,128)(2,1)S(1)} %copy-done.2, f32[2048]{0:T(1024)S(1)} %copy-done.5, ...), kind=kOutput, calls=%fused_computation.17 | convolution fusion | flops 4436361216 | bytes 16852480 | tf_op jit(solution)/shard_map/dot_general | solution.py:83
  503.6 26.4 %reduce-scatter.5.cloned.1.call-done = bf16[512,384]{0,1:T(8,128)(2,1)} async-done(((bf16[2048,384]{0,1:T(8,128)(2,1)}), bf16[512,384]{0,1:T(8,128)(2,1)}) %reduce-scatter.5.cloned.1.call-update) | async-done | bytes 393232 | tf_op jit(solution)/shard_map/reduce_scatter | solution.py:82
  530.1 1.1 add_convert_fusion
  531.2 0.9 copy.13
  (30 shorter events, 0.5 us)
Async XLA Ops:
  6.5 54.3 %copy-start.4 = (f32[2048]{0:T(1024)S(1)}, f32[2048]{0:T(1024)}, u32[]{:S(2)}) copy-start(f32[2048]{0:T(1024)} %param.12) | copy-start | bytes 24580
  6.5 24.7 %all-gather.9.cloned.1.call-start = ((), (), s32[]{:S(2)}) async-start(), calls=%async_computation.2 | async-start | bytes 1966080 | tf_op jit(solution)/shard_map/all_gather | solution.py:39
  7.3 53.6 %all-gather.13.cloned.1.call-start = ((), (), s32[]{:S(2)}) async-start(), calls=%async_computation.4 | async-start | bytes 1310720 | tf_op jit(solution)/shard_map/all_gather | solution.py:43
  8.0 81.8 %all-gather.11.cloned.1.call-start = ((), (), s32[]{:S(2)}) async-start(), calls=%async_computation.3 | async-start | bytes 1310720 | tf_op jit(solution)/shard_map/all_gather | solution.py:42
  8.7 109.9 %all-gather.15.cloned.1.call-start = ((), (), s32[]{:S(2)}) async-start(), calls=%async_computation.5 | async-start | bytes 1310720 | tf_op jit(solution)/shard_map/all_gather | solution.py:44
  9.3 140.0 %reduce-scatter.3.cloned.1.call-start = ((), (), s32[]{:S(2)}) async-start(), calls=%async_computation.6 | async-start | bytes 1966080 | tf_op jit(solution)/shard_map/reduce_scatter | solution.py:64
  33.1 56.7 %copy-start.1 = (bf16[2048,384]{1,0:T(8,128)(2,1)S(1)}, bf16[2048,384]{1,0:T(8,128)(2,1)}, u32[]{:S(2)}) copy-start(bf16[2048,384]{1,0:T(8,128)(2,1)} %all-gather.9.cloned.1.call-done) | copy-start | bytes 4718596
  118.6 3.2 copy-start.3
  121.8 49.2 %all-gather.17.cloned.1.call-start = ((), (), s32[]{:S(2)}) async-start(), calls=%async_computation.7 | async-start | bytes 1966080 | tf_op jit(solution)/shard_map/all_gather | solution.py:72
  151.1 128.1 %all-gather.19.cloned.1.call-start = ((), (), s32[]{:S(2)}) async-start(), calls=%async_computation.8 | async-start | bytes 7208960 | tf_op jit(solution)/shard_map/all_gather | solution.py:75
  151.9 127.3 %copy-start.5 = (f32[2048]{0:T(1024)S(1)}, f32[2048]{0:T(1024)}, u32[]{:S(2)}) copy-start(f32[2048]{0:T(1024)} %param.18) | copy-start | bytes 24580
  151.9 233.9 %all-gather.21.cloned.1.call-start = ((), (), s32[]{:S(2)}) async-start(), calls=%async_computation.9 | async-start | bytes 7208960 | tf_op jit(solution)/shard_map/all_gather | solution.py:76
  152.7 339.7 %all-gather.23.cloned.1.call-start = ((), (), s32[]{:S(2)}) async-start(), calls=%async_computation.10 | async-start | bytes 7208960 | tf_op jit(solution)/shard_map/all_gather | solution.py:81
  153.4 376.7 %reduce-scatter.5.cloned.1.call-start = ((), (), s32[]{:S(2)}) async-start(), calls=%async_computation.11 | async-start | bytes 1966080 | tf_op jit(solution)/shard_map/reduce_scatter | solution.py:82
  172.7 319.6 %copy-start.2 = (bf16[2048,384]{0,1:T(8,128)(2,1)S(1)}, bf16[2048,384]{0,1:T(8,128)(2,1)}, u32[]{:S(2)}) copy-start(bf16[2048,384]{0,1:T(8,128)(2,1)} %all-gather.17.cloned.1.call-done) | copy-start | bytes 4718596
  286.4 243.7 %copy-start = (bf16[512,384]{0,1:T(8,128)(2,1)S(1)}, bf16[512,384]{0,1:T(8,128)(2,1)}, u32[]{:S(2)}) copy-start(bf16[512,384]{0,1:T(8,128)(2,1)} %add_convert_fusion.1) | copy-start | bytes 1179652
Sparse Core Ops, SparseCore 0:
  8.9 22.3 all-gather.8
  32.8 27.9 all-gather.12
  62.4 27.3 all-gather.10
  91.3 27.3 all-gather.14
  121.9 27.3 reduce-scatter.2
  151.3 19.6 all-gather.16
  172.5 106.6 all-gather.18
  280.8 104.9 all-gather.20
  387.4 104.9 all-gather.22
  503.8 26.2 reduce-scatter.4
where the time goes:
time: 539 us
  waiting for transfers between devices  482 us (89%)
  matrix products  26.5 us (5%)
  between operations  13.6 us (3%)
  other arithmetic  8.9 us (2%)
  blocking collectives  6.08 us (1%)
    all_gather x1, waiting for transfers between devices, on_device(): down_whole = lax.all_gather(ffn_down, 'fs', axis=0, tiled=True)  107 us
    all_gather x1, waiting for transfers between devices, on_device(): lax.all_gather(ffn_gate, 'fs', axis=0, tiled=True)  106 us
    all_gather x1, waiting for transfers between devices, on_device(): lax.all_gather(ffn_up, 'fs', axis=0, tiled=True)  99.4 us
    all_gather x1, waiting for transfers between devices, on_device(): lax.all_gather(glu_gate, 'fs', axis=0, tiled=True)  27.8 us
    reduce_scatter x1, waiting for transfers between devices, on_device(): lax.psum_scatter(jnp.dot(out_w, activated, preferred_element_type=jnp.flo...  27.2 us
    reduce_scatter x1, waiting for transfers between devices, on_device(): lax.psum_scatter(jnp.dot(down_whole, hidden, preferred_element_type=jnp.f...  26.4 us
    all_gather x1, waiting for transfers between devices, on_device(): lax.all_gather(glu_value, 'fs', axis=0, tiled=True)  26.2 us
    all_gather x1, waiting for transfers between devices, on_device(): gathered = lax.all_gather(stream, 'tp', axis=0, tiled=True)  20.4 us
  transfers between devices with their start and end apart: 10, of which 10 were waited for; matrix products, arithmetic and copies ran while one was open for 4% of the time, Pallas kernels for 0%

commit v1 on v0

v1 whole, which is shorter than its diff:
```python
import functools

import jax
import jax.numpy as jnp
from jax import lax
from jax.experimental import pallas as pl
from jax.experimental.pallas import tpu as pltpu
from jax.sharding import PartitionSpec as P

MESH = pl.DeviceIdType.MESH
NT = (((1,), (1,)), ((), ()))
FIRST = 4


def layer_kernel(
    n_grp, n_fs, n_tp, pieces, total_channels,
    stream, w0, w1, w2, w3, w4, w5,
    mixer_gain, conv_kernel, channel_gain, ffn_gain,
    out,
    b0, b1, b2, b3, b4, b5,
    x_all, x_wide, x_norm, padded, stat_out, stat_in,
    part_one, got_one, middle_all, acc, hidden, part_two, got_two,
    z_recv, y_recv, left_send, right_send, y_send, own_sem,
    x_recv, x_send, st_recv, st_send,
    p1_recv, p1_send, m_recv, m_send, p2_recv, p2_send,
):
    y = lax.axis_index("grp")
    f = lax.axis_index("fs")
    t = lax.axis_index("tp")
    weights = (w0, w1, w2, w3, w4, w5)
    bufs = (b0, b1, b2, b3, b4, b5)
    feats, length = stream.shape
    width = feats * n_tp
    per = n_fs // n_tp
    rows = width // n_fs

    def tp_peer(k):
        return lax.rem(t + k, n_tp)

    barrier = pltpu.get_barrier_semaphore()
    for k in range(1, n_tp):
        pl.semaphore_signal(barrier, inc=1, device_id={"tp": tp_peer(k)}, device_id_type=MESH)
    for k in range(1, n_grp):
        pl.semaphore_signal(
            barrier, inc=1, device_id={"grp": lax.rem(y + k, n_grp)}, device_id_type=MESH
        )

    @pl.when(f > 0)
    def _():
        pl.semaphore_signal(barrier, inc=1, device_id={"fs": f - 1}, device_id_type=MESH)

    @pl.when(f < n_fs - 1)
    def _():
        pl.semaphore_signal(barrier, inc=1, device_id={"fs": f + 1}, device_id_type=MESH)

    ends = (f + n_fs - 1) // n_fs + (2 * (n_fs - 1) - f) // n_fs
    pl.semaphore_wait(barrier, n_tp - 1 + n_grp - 1 + ends)

    def remote(src, dst, send, recv, where):
        return pltpu.make_async_remote_copy(
            src_ref=src, dst_ref=dst, send_sem=send, recv_sem=recv,
            device_id=where, device_id_type=MESH,
        )

    def slot(c, s, half):
        w, u, subs = pieces[c]
        return bufs[w].at[s, half * subs + u]

    def own_src(c):
        w, u, subs = pieces[c]
        size = bufs[w].shape[2]
        start = pl.multiple_of((y * subs + u) * size, size)
        return weights[w].at[pl.ds(start, size)]

    def z_copy(c, s, step, src=None):
        here = slot(c, s, y)
        sems = right_send if step > 0 else left_send
        return remote(
            here if src is None else src, here, sems.at[c, s], z_recv.at[c, s], {"fs": f + step}
        )

    def y_copy(c, s, half):
        here = slot(c, s, half)
        return remote(
            here, here, y_send.at[c, s], y_recv.at[c, s], {"grp": lax.rem(y + 1, n_grp)}
        )

    def send_own(c):
        @pl.when(f > 0)
        def _():
            z_copy(c, f, -1, own_src(c)).start()

        @pl.when(f < n_fs - 1)
        def _():
            z_copy(c, f, 1, own_src(c)).start()

    def each_distance(body):
        if n_fs <= 4:
            for d in range(1, n_fs):
                body(d)
        else:
            lax.fori_loop(1, n_fs, lambda d, carry: (body(d), carry)[1], 0)

    def forward(c, d):
        @pl.when(f - d >= 0)
        def _():
            s = jnp.maximum(f - d, 0)
            z_copy(c, s, 1).wait_recv()

            @pl.when(f < n_fs - 1)
            def _():
                z_copy(c, s, 1).start()

            y_copy(c, s, y).start()

        @pl.when(f + d < n_fs)
        def _():
            s = jnp.minimum(f + d, n_fs - 1)
            z_copy(c, s, -1).wait_recv()

            @pl.when(f > 0)
            def _():
                z_copy(c, s, -1).start()

            y_copy(c, s, y).start()

    def other_half(c, s):
        y_copy(c, s, lax.rem(y + 1, n_grp)).wait_recv()

    def other_halves(cs, d):
        @pl.when(f - d >= 0)
        def _():
            for c in cs:
                other_half(c, jnp.maximum(f - d, 0))

        @pl.when(f + d < n_fs)
        def _():
            for c in cs:
                other_half(c, jnp.minimum(f + d, n_fs - 1))

    count = len(pieces)
    of = [[c for c in range(count) if pieces[c][0] == w] for w in range(6)]
    glue = of[0] + of[1] + of[2]

    x_copies = []
    for k in range(1, n_tp):
        x_copies.append(
            remote(stream, x_all.at[t], x_send.at[k], x_recv.at[t], {"tp": tp_peer(k)})
        )
        x_copies[-1].start()
    for c in range(FIRST):
        send_own(c)
    x_own = pltpu.make_async_copy(stream, x_all.at[t], own_sem.at[0])
    x_own.start()
    owns = []
    for w in range(6):
        parts, size = bufs[w].shape[1], bufs[w].shape[2]
        for p in range(parts):
            owns.append(
                pltpu.make_async_copy(
                    weights[w].at[pl.ds(p * size, size)], bufs[w].at[f, p],
                    own_sem.at[1 + len(owns)],
                )
            )
            owns[-1].start()
    padded[pl.ds(0, 32), :] = jnp.zeros((32, padded.shape[1]), jnp.float32)

    def normalize(source, gain):
        for start in range(0, length, 128):
            tokens = pl.ds(start, 128)
            total = jnp.zeros((128, 1), jnp.float32)
            for b in range(n_tp):
                block = source[b, :, tokens].astype(jnp.float32).T
                x_wide[b, tokens, :] = block
                total = total + jnp.sum(block * block, axis=1, keepdims=True)
            inverse = lax.rsqrt(total / width + 1e-06)
            for b in range(n_tp):
                scaled = x_wide[b, tokens, :] * inverse * gain[:, pl.ds(b * feats, feats)]
                scaled = scaled.astype(jnp.bfloat16)
                for j in range(per):
                    x_norm[b * per + j, tokens, :] = scaled[:, j * rows : (j + 1) * rows]

    def weight_block(w, s, columns):
        block = bufs[w][s, :, :, columns]
        return block.reshape(rows, block.shape[-1])

    for c in glue:
        forward(c, 1)
    for k in range(1, n_tp):
        src = tp_peer(k)
        remote(
            stream, x_all.at[src], x_send.at[k], x_recv.at[src], {"tp": src}
        ).wait_recv()
    x_own.wait()
    normalize(x_all, mixer_gain)

    def rest(d):
        for c in glue:
            forward(c, d)

    if n_fs <= 4:
        for d in range(2, n_fs):
            rest(d)
    else:
        lax.fori_loop(2, n_fs, lambda d, carry: (rest(d), carry)[1], 0)
    for c in range(FIRST, count):
        send_own(c)
    forward(of[3][0], 1)
    for copy in owns:
        copy.wait()
    each_distance(lambda d: other_halves(of[0] + of[1], d))

    channels = w0.shape[1]
    everything = pl.ds(0, channels)

    def project(w, columns):
        def add(s, total):
            return total + jnp.dot(
                x_norm[s], weight_block(w, s, columns), preferred_element_type=jnp.float32
            )

        return lax.fori_loop(0, n_fs, add, jnp.zeros((length, columns.size), jnp.float32))

    value_part = project(0, everything)
    gate_part = project(1, everything)
    gated = (value_part * jax.nn.sigmoid(gate_part)).astype(jnp.bfloat16)
    padded[pl.ds(32, length), :] = gated.astype(jnp.float32)

    mine = pl.ds(pl.multiple_of(t * channels, channels), channels)
    taps = conv_kernel[:, mine].astype(jnp.float32)
    n_taps = conv_kernel.shape[0]
    lane = lax.broadcasted_iota(jnp.int32, (128, 128), 1)
    conv = []
    for start in range(0, length, 128):
        total = jnp.zeros((128, channels), jnp.float32)
        for k in range(n_taps):
            total = total + taps[k : k + 1, :] * padded[
                pl.ds(start + 32 - (n_taps - 1) + k, 128), :
            ]
        conv.append(total)
        sums = jnp.sum(total, axis=1, keepdims=True)
        squares = jnp.sum(total * total, axis=1, keepdims=True)
        both = jnp.where(lane == 0, sums, jnp.where(lane == 1, squares, 0.0))
        stat_out[:, pl.ds(start, 128)] = both.T[:8, :]

    for k in range(1, n_tp):
        remote(
            stat_out, stat_in.at[t], st_send.at[k], st_recv.at[t], {"tp": tp_peer(k)}
        ).start()
    for c in of[3]:
        if c != of[3][0]:
            forward(c, 1)
    each_distance(lambda d: other_halves(of[2], d))
    for k in range(1, n_tp):
        src = tp_peer(k)
        remote(
            stat_out, stat_in.at[src], st_send.at[k], st_recv.at[src], {"tp": src}
        ).wait_recv()
    stats = stat_out[...]
    for k in range(1, n_tp):
        stats = stats + stat_in[tp_peer(k)]
    activated = []
    for i, start in enumerate(range(0, length, 128)):
        turned = jnp.concatenate(
            [stats[:, start : start + 128], jnp.zeros((120, 128), jnp.float32)], axis=0
        ).T
        mean_val = turned[:, 0:1] / total_channels
        mean_sq = turned[:, 1:2] / total_channels
        scaled = (
            (conv[i] - mean_val)
            * lax.rsqrt(mean_sq - mean_val * mean_val + 1e-05)
            * channel_gain[:, mine]
        )
        activated.append(jax.nn.silu(scaled).astype(jnp.bfloat16))
    activated = jnp.concatenate(activated, axis=0)

    def share(part, got, p_send, p_recv, s):
        dest = s // per
        return remote(
            part.at[s], got.at[t, lax.rem(s, per)], p_send.at[s],
            p_recv.at[t, lax.rem(s, per)], {"tp": dest},
        )

    def send_share(part, got, p_send, p_recv, s):
        @pl.when(s // per != t)
        def _():
            share(part, got, p_send, p_recv, s).start()

    def collect(part, got, p_send, p_recv, base, store):
        for k in range(1, n_tp):
            src = tp_peer(k)
            for j in range(per):
                remote(
                    part.at[j], got.at[src, j], p_send.at[j], p_recv.at[src, j], {"tp": src}
                ).wait_recv()
        for j in range(per):
            here = pl.ds(j * rows, rows)
            total = part[t * per + j].astype(jnp.float32)
            for k in range(1, n_tp):
                total = total + got[tp_peer(k), j].astype(jnp.float32)
            store(here, base[here, :].astype(jnp.float32) + total)

    def mix(s, carry):
        part_one[s] = lax.dot_general(
            weight_block(2, s, everything), activated, NT, preferred_element_type=jnp.float32
        ).astype(jnp.bfloat16)
        send_share(part_one, got_one, p1_send, p1_recv, s)
        return carry

    lax.fori_loop(0, n_fs, mix, 0)

    def many(cs, first, last):
        def go(d):
            for c in cs:
                forward(c, d)

        if n_fs <= 4:
            for d in range(first, last):
                go(d)
        else:
            lax.fori_loop(first, last, lambda d, carry: (go(d), carry)[1], 0)

    many(of[3], 2, n_fs - 1)

    def keep_middle(here, value):
        middle_all[t, here, :] = value.astype(jnp.bfloat16)

    collect(part_one, got_one, p1_send, p1_recv, x_all.at[t], keep_middle)
    for k in range(1, n_tp):
        remote(
            middle_all.at[t], middle_all.at[t], m_send.at[k], m_recv.at[t], {"tp": tp_peer(k)}
        ).start()
    many(of[3], n_fs - 1, n_fs)
    for c in of[4]:
        forward(c, 1)
    for k in range(1, n_tp):
        src = tp_peer(k)
        remote(
            middle_all.at[src], middle_all.at[src], m_send.at[k], m_recv.at[src], {"tp": src}
        ).wait_recv()
    normalize(middle_all, ffn_gain)
    many(of[4], 2, n_fs - 1)
    each_distance(lambda d: other_halves(of[3], d))

    units = w3.shape[1]
    tiles = [pl.ds(a, min(256, units - a)) for a in range(0, units, 256)]
    for columns in tiles:
        acc[:, columns] = project(3, columns)
    many(of[4], n_fs - 1, n_fs)
    for c in of[5]:
        forward(c, 1)
    each_distance(lambda d: other_halves(of[4], d))
    for columns in tiles:
        hidden[:, columns] = (jax.nn.silu(acc[:, columns]) * project(4, columns)).astype(
            jnp.bfloat16
        )

    def down(s):
        block = bufs[5][s].reshape(rows, units)
        part_two[s] = lax.dot_general(
            block, hidden[...], NT, preferred_element_type=jnp.float32
        ).astype(jnp.bfloat16)
        send_share(part_two, got_two, p2_send, p2_recv, s)

    def down_at(d):
        other_halves(of[5], d)

        def both(i, carry):
            s = f + d - 2 * d * i

            @pl.when(jnp.logical_and(s >= 0, s < n_fs))
            def _():
                down(jnp.clip(s, 0, n_fs - 1))

            return carry

        lax.fori_loop(0, 2, both, 0)

    down(f)

    def last(d):
        for c in of[5]:
            forward(c, d)
        down_at(d - 1)

    if n_fs <= 4:
        for d in range(2, n_fs):
            last(d)
    else:
        lax.fori_loop(2, n_fs, lambda d, carry: (last(d), carry)[1], 0)
    down_at(n_fs - 1)

    def keep_result(here, value):
        out[here, :] = value.astype(jnp.bfloat16)

    collect(part_two, got_two, p2_send, p2_recv, middle_all.at[t], keep_result)

    for copy in x_copies:
        copy.wait_send()
    for k in range(1, n_tp):
        remote(
            stat_out, stat_in.at[t], st_send.at[k], st_recv.at[t], {"tp": tp_peer(k)}
        ).wait_send()
        remote(
            middle_all.at[t], middle_all.at[t], m_send.at[k], m_recv.at[t], {"tp": tp_peer(k)}
        ).wait_send()

    def drain(s, carry):
        @pl.when(s // per != t)
        def _():
            share(part_one, got_one, p1_send, p1_recv, s).wait_send()
            share(part_two, got_two, p2_send, p2_recv, s).wait_send()

        for c in range(count):
            @pl.when(jnp.logical_and(s <= f, f < n_fs - 1))
            def _():
                z_copy(c, s, 1).wait_send()

            @pl.when(jnp.logical_and(s >= f, f > 0))
            def _():
                z_copy(c, s, -1).wait_send()

            @pl.when(s != f)
            def _():
                y_copy(c, s, y).wait_send()

        return carry

    lax.fori_loop(0, n_fs, drain, 0)


def on_device(sizes, *args):
    (stream, mixer_gain, glu_value, glu_gate, conv_kernel, channel_gain,
     conv_out, ffn_gain, ffn_gate, ffn_up, ffn_down) = args
    n_grp, n_fs, n_tp = sizes
    weights = (glu_value, glu_gate, conv_out, ffn_gate, ffn_up, ffn_down)
    feats, length = stream.shape
    width = feats * n_tp
    rows = width // n_fs
    channels = glu_value.shape[1]
    units = ffn_gate.shape[1]
    pieces, bufs = [], []
    for w, weight in enumerate(weights):
        subs = 2 if (w >= 3 and n_fs <= 4) else 1
        pieces += [(w, u, subs) for u in range(subs)]
        bufs.append(
            pltpu.VMEM(
                (n_fs, n_grp * subs, rows // (n_grp * subs), weight.shape[1]), jnp.bfloat16
            )
        )
    count = len(pieces)
    per = n_fs // n_tp
    any_spec = pl.BlockSpec(memory_space=pl.ANY)
    vmem = pl.BlockSpec(memory_space=pltpu.VMEM)
    dma = pltpu.SemaphoreType.DMA
    owns = 1 + sum(buf.shape[1] for buf in bufs)
    return pl.pallas_call(
        functools.partial(
            layer_kernel, n_grp, n_fs, n_tp, tuple(pieces), channel_gain.shape[0]
        ),
        out_shape=jax.ShapeDtypeStruct((feats, length), jnp.bfloat16),
        in_specs=[any_spec] * 7 + [vmem] * 4,
        out_specs=vmem,
        scratch_shapes=bufs
        + [
            pltpu.VMEM((n_tp, feats, length), jnp.bfloat16),
            pltpu.VMEM((n_tp, length, feats), jnp.float32),
            pltpu.VMEM((n_fs, length, rows), jnp.bfloat16),
            pltpu.VMEM((length + 32, channels), jnp.float32),
            pltpu.VMEM((8, length), jnp.float32),
            pltpu.VMEM((n_tp, 8, length), jnp.float32),
            pltpu.VMEM((n_fs, rows, length), jnp.bfloat16),
            pltpu.VMEM((n_tp, per, rows, length), jnp.bfloat16),
            pltpu.VMEM((n_tp, feats, length), jnp.bfloat16),
            pltpu.VMEM((length, units), jnp.float32),
            pltpu.VMEM((length, units), jnp.bfloat16),
            pltpu.VMEM((n_fs, rows, length), jnp.bfloat16),
            pltpu.VMEM((n_tp, per, rows, length), jnp.bfloat16),
        ]
        + [dma((count, n_fs))] * 5
        + [dma((owns,))]
        + [dma((n_tp,))] * 4
        + [dma((n_tp, per)), dma((n_fs,))]
        + [dma((n_tp,))] * 2
        + [dma((n_tp, per)), dma((n_fs,))],
        compiler_params=pltpu.CompilerParams(
            collective_id=0, has_side_effects=True, vmem_limit_bytes=62 * 1024 * 1024
        ),
    )(
        stream, *weights, mixer_gain[None, :], conv_kernel, channel_gain[None, :],
        ffn_gain[None, :],
    )


def solution(mesh):
    in_specs = (
        P("tp", ("grp", "fs")),
        P(),
        P("fs", "tp"),
        P("fs", "tp"),
        P(),
        P(),
        P("fs", "tp"),
        P(),
        P("fs", "tp"),
        P("fs", "tp"),
        P("fs", "tp"),
    )
    sizes = (mesh.shape["grp"], mesh.shape["fs"], mesh.shape["tp"])
    return jax.shard_map(
        functools.partial(on_device, sizes), mesh=mesh, in_specs=in_specs,
        out_specs=P("tp", ("grp", "fs")), check_vma=False,
    )
```

time: 539 us -> 224 us (0.42)
  waiting for transfers between devices: 482 us -> 0 us
  Pallas kernels: 0 us -> 222 us
  matrix products: 26.5 us -> 0 us
  between operations: 13.6 us -> 0.01 us
  other arithmetic: 8.9 us -> 0 us
  blocking collectives: 6.08 us -> 0 us
    all_gather x8 -> x0, waiting for transfers between devices: 423 us -> none  [the longest x1 107 us: on_device(): down_whole = lax.all_gather(ffn_down, 'fs', axis=0, tiled=True)]
    pallas_call x0 -> x1, Pallas kernels: none -> 222 us  [on_device(): pl.pallas_call(functools.partial(layer_kernel, n_grp, n_fs, n_tp, tuple(p...]
    reduce_scatter x2 -> x0, waiting for transfers between devices: 53.7 us -> none  [the longest x1 27.2 us: on_device(): lax.psum_scatter(jnp.dot(out_w, activated, preferred_element_type=jnp.flo...]
    dot_general x5 -> x0, matrix products: 26.5 us -> none  [the longest x3 12.1 us: contract(): lax.dot_general(weight, acts, (((0,), (0,)), ((), ())), preferred_element...]
    psum x1 -> x0, blocking collectives: 6.08 us -> none  [on_device(): lax.psum((jnp.sum(conv_sum, axis=0), jnp.sum(conv_sum * conv_sum, axis=0)...]
  transfers between devices with their start and end apart: 10 -> 0, of which waited for: 10 -> 0; matrix products, arithmetic and copies ran while one was open for 4% -> 0% of each run, Pallas kernels for 0% -> 0%
where the time goes in v1:
time: 224 us
  Pallas kernels  222 us (99%)
    pallas_call x1, Pallas kernels, on_device(): pl.pallas_call(functools.partial(layer_kernel, n_grp, n_fs, n_tp, tuple(p...  222 us

profile of v1, /device:TPU:0, one launch (start us, length us, event | category | flops | bytes accessed | tf_op | source)
XLA Modules:
  0.0 224.0 jit_solution(9042521763317890583)
XLA Ops:
  0.0 222.2 %shard_map.109 = bf16[512,384]{1,0:T(8,128)(2,1)} custom-call(bf16[512,384]{1,0:T(8,128)(2,1)} %stream.1, bf16[512,256]{1,0:T(8,128)(2,1)} %w0.1, bf16[512,256]{1,0:T(8,128)(2,1)} %w1.1, bf16[512,256]{1,0:T(8,128)(2,1)} %w2.1, bf16[512,1408]{1,0:T(8,128)(2,1)} %w3.1, bf16[512,1408]{1,0:T(8,128)(2,1)} %w4.1, bf16[512,1408]{1,0:T(8,128)(2,1)} %w5.1, ...), custom_call_target="tpu_custom_call" | custom-call | tf_op jit(solution)/shard_map/pallas_call | solution.py:457
  222.2 1.8 copy.13

commit v2 on v1

--- a/solution.py
+++ b/solution.py
@@ -20,7 +20,8 @@
     b0, b1, b2, b3, b4, b5,
     x_all, x_wide, x_norm, padded, stat_out, stat_in,
     part_one, got_one, middle_all, acc, hidden, part_two, got_two,
-    z_recv, y_recv, left_send, right_send, y_send, own_sem,
+    returned, back,
+    z_recv, y_recv, left_send, right_send, y_send, own_sem, g_sem,
     x_recv, x_send, st_recv, st_send,
     p1_recv, p1_send, m_recv, m_send, p2_recv, p2_send,
 ):
@@ -34,6 +35,10 @@
     per = n_fs // n_tp
     rows = width // n_fs
 
+    inner = jnp.logical_and(f > 0, f < n_fs - 1)
+    guest = jnp.logical_or(f == 1, f == n_fs - 2)
+    toward = jnp.where(f == 0, 1, -1)
+
     def tp_peer(k):
         return lax.rem(t + k, n_tp)
 
@@ -66,10 +71,13 @@
         w, u, subs = pieces[c]
         return bufs[w].at[s, half * subs + u]
 
-    def own_src(c):
+    def is_ffn(c):
+        return pieces[c][0] >= 3
+
+    def own_src(c, half):
         w, u, subs = pieces[c]
         size = bufs[w].shape[2]
-        start = pl.multiple_of((y * subs + u) * size, size)
+        start = pl.multiple_of((half * subs + u) * size, size)
         return weights[w].at[pl.ds(start, size)]
 
     def z_copy(c, s, step, src=None):
@@ -79,20 +87,42 @@
             here if src is None else src, here, sems.at[c, s], z_recv.at[c, s], {"fs": f + step}
         )
 
+    def other_y():
+        return lax.rem(y + 1, n_grp)
+
+    def z_extra(c, step):
+        return remote(
+            own_src(c, other_y()), slot(c, f, other_y()), y_send.at[c, f], y_recv.at[c, f],
+            {"fs": f + step},
+        )
+
     def y_copy(c, s, half):
         here = slot(c, s, half)
-        return remote(
-            here, here, y_send.at[c, s], y_recv.at[c, s], {"grp": lax.rem(y + 1, n_grp)}
-        )
+        return remote(here, here, y_send.at[c, s], y_recv.at[c, s], {"grp": other_y()})
+
+    def goes_left(c):
+        return f > (1 if is_ffn(c) else 0)
+
+    def goes_right(c):
+        return f < (n_fs - 2 if is_ffn(c) else n_fs - 1)
 
     def send_own(c):
-        @pl.when(f > 0)
-        def _():
-            z_copy(c, f, -1, own_src(c)).start()
-
-        @pl.when(f < n_fs - 1)
-        def _():
-            z_copy(c, f, 1, own_src(c)).start()
+        @pl.when(goes_left(c))
+        def _():
+            z_copy(c, f, -1, own_src(c, y)).start()
+
+        @pl.when(goes_right(c))
+        def _():
+            z_copy(c, f, 1, own_src(c, y)).start()
+
+        if is_ffn(c):
+            @pl.when(f == 0)
+            def _():
+                z_extra(c, 1).start()
+
+            @pl.when(f == n_fs - 1)
+            def _():
+                z_extra(c, -1).start()
 
     def each_distance(body):
         if n_fs <= 4:
@@ -101,31 +131,48 @@
         else:
             lax.fori_loop(1, n_fs, lambda d, carry: (body(d), carry)[1], 0)
 
+    def by_y(c, s):
+        if not is_ffn(c):
+            return s != f
+        near = jnp.logical_or(
+            jnp.logical_and(s == 0, f == 1), jnp.logical_and(s == n_fs - 1, f == n_fs - 2)
+        )
+        return jnp.logical_and(jnp.logical_and(inner, s != f), jnp.logical_not(near))
+
     def forward(c, d):
-        @pl.when(f - d >= 0)
+        from_left, from_right = f - d >= 0, f + d < n_fs
+        if is_ffn(c):
+            from_left = jnp.logical_and(from_left, inner)
+            from_right = jnp.logical_and(from_right, inner)
+
+        @pl.when(from_left)
         def _():
             s = jnp.maximum(f - d, 0)
             z_copy(c, s, 1).wait_recv()
 
-            @pl.when(f < n_fs - 1)
+            @pl.when(goes_right(c))
             def _():
                 z_copy(c, s, 1).start()
 
-            y_copy(c, s, y).start()
-
-        @pl.when(f + d < n_fs)
+            @pl.when(by_y(c, s))
+            def _():
+                y_copy(c, s, y).start()
+
+        @pl.when(from_right)
         def _():
             s = jnp.minimum(f + d, n_fs - 1)
             z_copy(c, s, -1).wait_recv()
 
-            @pl.when(f > 0)
+            @pl.when(goes_left(c))
             def _():
                 z_copy(c, s, -1).start()
 
-            y_copy(c, s, y).start()
+            @pl.when(by_y(c, s))
+            def _():
+                y_copy(c, s, y).start()
 
     def other_half(c, s):
-        y_copy(c, s, lax.rem(y + 1, n_grp)).wait_recv()
+        y_copy(c, s, other_y()).wait_recv()
 
     def other_halves(cs, d):
         @pl.when(f - d >= 0)
@@ -152,20 +199,28 @@
         send_own(c)
     x_own = pltpu.make_async_copy(stream, x_all.at[t], own_sem.at[0])
     x_own.start()
-    owns = []
+    owns, ffn_owns = [], []
     for w in range(6):
         parts, size = bufs[w].shape[1], bufs[w].shape[2]
         for p in range(parts):
-            owns.append(
+            kept = owns if w < 3 else ffn_owns
+            kept.append(
                 pltpu.make_async_copy(
                     weights[w].at[pl.ds(p * size, size)], bufs[w].at[f, p],
-                    own_sem.at[1 + len(owns)],
+                    own_sem.at[1 + len(owns) + len(ffn_owns)],
                 )
             )
-            owns[-1].start()
+    for copy in owns:
+        copy.start()
+
+    @pl.when(inner)
+    def _():
+        for copy in ffn_owns:
+            copy.start()
+
     padded[pl.ds(0, 32), :] = jnp.zeros((32, padded.shape[1]), jnp.float32)
 
-    def normalize(source, gain):
+    def normalize(source, gain, base=0):
         for start in range(0, length, 128):
             tokens = pl.ds(start, 128)
             total = jnp.zeros((128, 1), jnp.float32)
@@ -178,7 +233,7 @@
                 scaled = x_wide[b, tokens, :] * inverse * gain[:, pl.ds(b * feats, feats)]
                 scaled = scaled.astype(jnp.bfloat16)
                 for j in range(per):
-                    x_norm[b * per + j, tokens, :] = scaled[:, j * rows : (j + 1) * rows]
+                    x_norm[b * per + j, pl.ds(base + start, 128), :] = scaled[:, j * rows : (j + 1) * rows]
 
     def weight_block(w, s, columns):
         block = bufs[w][s, :, :, columns]
@@ -204,7 +259,12 @@
     else:
         lax.fori_loop(2, n_fs, lambda d, carry: (rest(d), carry)[1], 0)
     for c in range(FIRST, count):
-        send_own(c)
+        if pieces[c][0] < 5:
+            send_own(c)
+        else:
+            @pl.when(inner)
+            def _():
+                send_own(c)
     forward(of[3][0], 1)
     for copy in owns:
         copy.wait()
@@ -213,10 +273,10 @@
     channels = w0.shape[1]
     everything = pl.ds(0, channels)
 
-    def project(w, columns):
+    def project(w, columns, base=0):
         def add(s, total):
             return total + jnp.dot(
-                x_norm[s], weight_block(w, s, columns), preferred_element_type=jnp.float32
+                x_norm[s, pl.ds(base, length), :], weight_block(w, s, columns), preferred_element_type=jnp.float32
             )
 
         return lax.fori_loop(0, n_fs, add, jnp.zeros((length, columns.size), jnp.float32))
@@ -323,44 +383,107 @@
     many(of[3], 2, n_fs - 1)
 
     def keep_middle(here, value):
-        middle_all[t, here, :] = value.astype(jnp.bfloat16)
+        middle_all[0, t, here, :] = value.astype(jnp.bfloat16)
 
     collect(part_one, got_one, p1_send, p1_recv, x_all.at[t], keep_middle)
-    for k in range(1, n_tp):
-        remote(
-            middle_all.at[t], middle_all.at[t], m_send.at[k], m_recv.at[t], {"tp": tp_peer(k)}
-        ).start()
+
+    def hand_over(step):
+        return remote(
+            middle_all.at[0, t], middle_all.at[1, t], g_sem.at[0], g_sem.at[1], {"fs": f + step}
+        )
+
+    def spread(g, k):
+        block = middle_all.at[g, t]
+        return remote(block, block, m_send.at[g, k], m_recv.at[g, t], {"tp": tp_peer(k)})
+
+    @pl.when(jnp.logical_not(inner))
+    def _():
+        hand_over(toward).start()
+        for c in of[5]:
+            send_own(c)
+
+    @pl.when(inner)
+    def _():
+        for k in range(1, n_tp):
+            spread(0, k).start()
+
     many(of[3], n_fs - 1, n_fs)
     for c in of[4]:
         forward(c, 1)
-    for k in range(1, n_tp):
-        src = tp_peer(k)
-        remote(
-            middle_all.at[src], middle_all.at[src], m_send.at[k], m_recv.at[src], {"tp": src}
-        ).wait_recv()
-    normalize(middle_all, ffn_gain)
+
+    @pl.when(guest)
+    def _():
+        hand_over(toward).wait_recv()
+        for k in range(1, n_tp):
+            spread(1, k).start()
+
     many(of[4], 2, n_fs - 1)
-    each_distance(lambda d: other_halves(of[3], d))
+
+    def gathered(g):
+        for k in range(1, n_tp):
+            src = tp_peer(k)
+            block = middle_all.at[g, src]
+            remote(block, block, m_send.at[g, k], m_recv.at[g, src], {"tp": src}).wait_recv()
+        normalize(middle_all.at[g], ffn_gain, g * length)
 
     units = w3.shape[1]
     tiles = [pl.ds(a, min(256, units - a)) for a in range(0, units, 256)]
-    for columns in tiles:
-        acc[:, columns] = project(3, columns)
+
+    def gates(g):
+        for columns in tiles:
+            acc[pl.ds(g * length, length), columns] = project(3, columns, g * length)
+
+    def ups(g):
+        for columns in tiles:
+            here = (pl.ds(g * length, length), columns)
+            hidden[here] = (
+                jax.nn.silu(acc[here]) * project(4, columns, g * length)
+            ).astype(jnp.bfloat16)
+
+    @pl.when(inner)
+    def _():
+        gathered(0)
+        each_distance(lambda d: other_halves(of[3], d))
+        for copy in ffn_owns:
+            copy.wait()
+        gates(0)
+
     many(of[4], n_fs - 1, n_fs)
     for c in of[5]:
         forward(c, 1)
-    each_distance(lambda d: other_halves(of[4], d))
-    for columns in tiles:
-        hidden[:, columns] = (jax.nn.silu(acc[:, columns]) * project(4, columns)).astype(
-            jnp.bfloat16
-        )
+
+    @pl.when(guest)
+    def _():
+        gathered(1)
+        gates(1)
+
+    many(of[5], 2, n_fs - 1)
+
+    @pl.when(inner)
+    def _():
+        each_distance(lambda d: other_halves(of[4], d))
+        ups(0)
+
+    @pl.when(guest)
+    def _():
+        ups(1)
+
+    def sums(g):
+        return part_two.at[g], got_two.at[g], p2_send.at[g], p2_recv.at[g]
 
     def down(s):
-        block = bufs[5][s].reshape(rows, units)
-        part_two[s] = lax.dot_general(
-            block, hidden[...], NT, preferred_element_type=jnp.float32
-        ).astype(jnp.bfloat16)
-        send_share(part_two, got_two, p2_send, p2_recv, s)
+        def one(g):
+            part_two[g, s] = lax.dot_general(
+                bufs[5][s].reshape(rows, units), hidden[pl.ds(g * length, length), :], NT,
+                preferred_element_type=jnp.float32,
+            ).astype(jnp.bfloat16)
+            send_share(*sums(g), s)
+
+        @pl.when(guest)
+        def _():
+            one(1)
+
+        one(0)
 
     def down_at(d):
         other_halves(of[5], d)
@@ -376,24 +499,45 @@
 
         lax.fori_loop(0, 2, both, 0)
 
-    down(f)
-
-    def last(d):
-        for c in of[5]:
-            forward(c, d)
-        down_at(d - 1)
-
-    if n_fs <= 4:
-        for d in range(2, n_fs):
-            last(d)
-    else:
-        lax.fori_loop(2, n_fs, lambda d, carry: (last(d), carry)[1], 0)
-    down_at(n_fs - 1)
-
-    def keep_result(here, value):
-        out[here, :] = value.astype(jnp.bfloat16)
-
-    collect(part_two, got_two, p2_send, p2_recv, middle_all.at[t], keep_result)
+    @pl.when(inner)
+    def _():
+        down(f)
+        if n_fs <= 4:
+            for d in range(1, n_fs - 2):
+                down_at(d)
+        else:
+            lax.fori_loop(1, n_fs - 2, lambda d, carry: (down_at(d), carry)[1], 0)
+
+    many(of[5], n_fs - 1, n_fs)
+
+    @pl.when(inner)
+    def _():
+        down_at(n_fs - 2)
+
+    def give_back(step):
+        return remote(returned, back, g_sem.at[2], g_sem.at[3], {"fs": f + step})
+
+    home = jnp.where(f == 1, -1, 1)
+
+    @pl.when(guest)
+    def _():
+        def keep(here, value):
+            returned[here, :] = value.astype(jnp.bfloat16)
+
+        collect(*sums(1), middle_all.at[1, t], keep)
+        give_back(home).start()
+
+    @pl.when(inner)
+    def _():
+        def keep(here, value):
+            out[here, :] = value.astype(jnp.bfloat16)
+
+        collect(*sums(0), middle_all.at[0, t], keep)
+
+    @pl.when(jnp.logical_not(inner))
+    def _():
+        give_back(home).wait_recv()
+        out[...] = back[...]
 
     for copy in x_copies:
         copy.wait_send()
@@ -401,26 +545,52 @@
         remote(
             stat_out, stat_in.at[t], st_send.at[k], st_recv.at[t], {"tp": tp_peer(k)}
         ).wait_send()
-        remote(
-            middle_all.at[t], middle_all.at[t], m_send.at[k], m_recv.at[t], {"tp": tp_peer(k)}
-        ).wait_send()
+
+    @pl.when(jnp.logical_not(inner))
+    def _():
+        hand_over(toward).wait_send()
+
+    @pl.when(inner)
+    def _():
+        for k in range(1, n_tp):
+            spread(0, k).wait_send()
+
+    @pl.when(guest)
+    def _():
+        for k in range(1, n_tp):
+            spread(1, k).wait_send()
+        give_back(home).wait_send()
 
     def drain(s, carry):
-        @pl.when(s // per != t)
+        away = s // per != t
+
+        @pl.when(away)
         def _():
             share(part_one, got_one, p1_send, p1_recv, s).wait_send()
-            share(part_two, got_two, p2_send, p2_recv, s).wait_send()
+
+        @pl.when(jnp.logical_and(away, inner))
+        def _():
+            share(*sums(0), s).wait_send()
+
+        @pl.when(jnp.logical_and(away, guest))
+        def _():
+            share(*sums(1), s).wait_send()
 
         for c in range(count):
-            @pl.when(jnp.logical_and(s <= f, f < n_fs - 1))
+            @pl.when(jnp.logical_and(s <= f, goes_right(c)))
             def _():
                 z_copy(c, s, 1).wait_send()
 
-            @pl.when(jnp.logical_and(s >= f, f > 0))
+            @pl.when(jnp.logical_and(s >= f, goes_left(c)))
             def _():
                 z_copy(c, s, -1).wait_send()
 
-            @pl.when(s != f)
+            sent = by_y(c, s)
+            if is_ffn(c):
+                own_end = jnp.logical_and(s == f, jnp.logical_not(inner))
+                sent = jnp.logical_or(sent, own_end)
+
+            @pl.when(sent)
             def _():
                 y_copy(c, s, y).wait_send()
 
@@ -465,24 +635,26 @@
         + [
             pltpu.VMEM((n_tp, feats, length), jnp.bfloat16),
             pltpu.VMEM((n_tp, length, feats), jnp.float32),
-            pltpu.VMEM((n_fs, length, rows), jnp.bfloat16),
+            pltpu.VMEM((n_fs, 2 * length, rows), jnp.bfloat16),
             pltpu.VMEM((length + 32, channels), jnp.float32),
             pltpu.VMEM((8, length), jnp.float32),
             pltpu.VMEM((n_tp, 8, length), jnp.float32),
             pltpu.VMEM((n_fs, rows, length), jnp.bfloat16),
             pltpu.VMEM((n_tp, per, rows, length), jnp.bfloat16),
-            pltpu.VMEM((n_tp, feats, length), jnp.bfloat16),
-            pltpu.VMEM((length, units), jnp.float32),
-            pltpu.VMEM((length, units), jnp.bfloat16),
-            pltpu.VMEM((n_fs, rows, length), jnp.bfloat16),
-            pltpu.VMEM((n_tp, per, rows, length), jnp.bfloat16),
+            pltpu.VMEM((2, n_tp, feats, length), jnp.bfloat16),
+            pltpu.VMEM((2 * length, units), jnp.float32),
+            pltpu.VMEM((2 * length, units), jnp.bfloat16),
+            pltpu.VMEM((2, n_fs, rows, length), jnp.bfloat16),
+            pltpu.VMEM((2, n_tp, per, rows, length), jnp.bfloat16),
+            pltpu.VMEM((feats, length), jnp.bfloat16),
+            pltpu.VMEM((feats, length), jnp.bfloat16),
         ]
         + [dma((count, n_fs))] * 5
-        + [dma((owns,))]
+        + [dma((owns,)), dma((4,))]
         + [dma((n_tp,))] * 4
         + [dma((n_tp, per)), dma((n_fs,))]
-        + [dma((n_tp,))] * 2
-        + [dma((n_tp, per)), dma((n_fs,))],
+        + [dma((2, n_tp))] * 2
+        + [dma((2, n_tp, per)), dma((2, n_fs))],
         compiler_params=pltpu.CompilerParams(
             collective_id=0, has_side_effects=True, vmem_limit_bytes=62 * 1024 * 1024
         ),

time: 224 us -> 187 us (0.83); the launches traced: 224 us -> 184 us
  Pallas kernels: 222 us -> 182 us
    pallas_call x1, Pallas kernels: 222 us -> 182 us  [on_device(): pl.pallas_call(functools.partial(layer_kernel, n_grp, n_fs, n_tp, tuple(p...]
where the time goes in v2:
time: 187 us; the launch traced here: 184 us
  Pallas kernels  182 us (97%)
    pallas_call x1, Pallas kernels, on_device(): pl.pallas_call(functools.partial(layer_kernel, n_grp, n_fs, n_tp, tuple(p...  182 us

profile of v2, /device:TPU:0, one launch (start us, length us, event | category | flops | bytes accessed | tf_op | source)
XLA Modules:
  0.0 184.2 jit_solution(11906245790053249670)
XLA Ops:
  0.0 182.4 %shard_map.109 = bf16[512,384]{1,0:T(8,128)(2,1)} custom-call(bf16[512,384]{1,0:T(8,128)(2,1)} %stream.1, bf16[512,256]{1,0:T(8,128)(2,1)} %w0.1, bf16[512,256]{1,0:T(8,128)(2,1)} %w1.1, bf16[512,256]{1,0:T(8,128)(2,1)} %w2.1, bf16[512,1408]{1,0:T(8,128)(2,1)} %w3.1, bf16[512,1408]{1,0:T(8,128)(2,1)} %w4.1, bf16[512,1408]{1,0:T(8,128)(2,1)} %w5.1, ...), custom_call_target="tpu_custom_call" | custom-call | tf_op jit(solution)/shard_map/pallas_call | solution.py:627
  182.4 1.8 copy.13
